TPU v7x, 32 devices: a whole 2x2x4 slice. The times are simulated.
32 devices in a mesh: ep: 32 (over z, y, x, core).
Axes of the slice: x: 2, y: 2, z: 4, core: 2. Of those that a mesh axis runs over, the one named last changes fastest.
Arguments:
- residual: bfloat16 [2048, 2048], P('ep'), may hold values from -6 to 6
- branch_in: bfloat16 [2048, 1024], P('ep'), may hold values from -6 to 6
- state_real: float32 [2048, 4096], P('ep'), may hold values from -4 to 4
- state_imag: float32 [2048, 4096], P('ep'), may hold values from -4 to 4
- decay_rate: float32 [64, 64], replicated, may hold values from 0.1 to 1
- frequency: float32 [64, 64], replicated, may hold values from 0 to 200
- log_step: float32 [64], replicated, may hold values from -4 to 0
- input_real: bfloat16 [64, 64, 16], replicated, may hold values from -1 to 1
- input_imag: bfloat16 [64, 64, 16], replicated, may hold values from -1 to 1
- output_matrix_real: bfloat16 [64, 16, 64], replicated, may hold values from -0.5 to 0.5
- output_matrix_imaginary: bfloat16 [64, 16, 64], replicated, may hold values from -0.5 to 0.5
- skip_gain: float32 [1024], replicated, may hold values from -4 to 4
- glu_value: bfloat16 [1024, 2048], replicated, may hold values from -0.1875 to 0.1875
- glu_gate: bfloat16 [1024, 2048], replicated, may hold values from -0.1875 to 0.1875
- mix_gain: float32 [2048], replicated, may hold values from 0.1 to 1.9
- moe_in_gain: float32 [2048], replicated, may hold values from 0.1 to 1.9
- moe_out_gain: float32 [2048], replicated, may hold values from 0.1 to 1.9
- routes: int32 [2048, 6], P('ep'), may hold values from 0 to 31, all different within a row; in each aligned block of 64 rows (0 to 63, 64 to 127, ...) at most 16 rows name the same one
- route_weights: float32 [2048, 6], P('ep'), may hold values from 0.05 to 0.6
- expert_gate: bfloat16 [32, 2048, 512], P('ep'), may hold values from -0.125 to 0.125
- expert_up: bfloat16 [32, 2048, 512], P('ep'), may hold values from -0.125 to 0.125
- expert_down: bfloat16 [32, 512, 2048], P('ep'), may hold values from -0.25 to 0.25
- shared_gate: bfloat16 [2048, 512], replicated, may hold values from -0.125 to 0.125
- shared_up: bfloat16 [2048, 512], replicated, may hold values from -0.125 to 0.125
- shared_down: bfloat16 [512, 2048], replicated, may hold values from -0.25 to 0.25
Outputs:
- layer_out: bfloat16 [2048, 2048], P('ep')
- next_real: float32 [2048, 4096], P('ep')
- next_imag: float32 [2048, 4096], P('ep')
Inputs may be any that keep to these rules, and one draw needn't show every extreme that they name: `routes`: among the rows of one device no expert is named more than 16 times, and in every draw some expert is named exactly 16 times by some device's rows; a token's experts are distinct.
All inputs are finite; a program needn't handle non-finite values.
Results may differ from a plain program's by a relative error of at most 0.0066.
Values may be sent and summed in bfloat16 or wider, within the bound.
A program may use at most 128 MiB of HBM per device.

v0:
```python
import functools

import jax
import jax.numpy as jnp
from jax import lax
from jax.experimental import pallas as pl
from jax.experimental.pallas import tpu as pltpu
from jax.sharding import PartitionSpec as P

norm_eps = 1e-06
ROW_TILE = 16
PIECES = 2
MESH = pl.DeviceIdType.MESH


def scaled_norm(row_block, norm_gain):
    return (
        row_block
        * lax.rsqrt(jnp.mean(row_block * row_block, axis=-1, keepdims=True) + norm_eps)
        * norm_gain
    )


def flipped(index, mask):
    out, bit = 0, 1
    while bit <= mask or bit == 1:
        digit = (index // bit) % 2
        out = out + bit * ((digit + 1) % 2 if mask & bit else digit)
        bit *= 2
    return out + (index // bit) * bit


def moe_kernel(
    planes,
    width,
    cap,
    normed,
    resid,
    slot_weights,
    out_gain,
    eg_hbm,
    eu_hbm,
    ed_hbm,
    sg_hbm,
    su_hbm,
    sd_hbm,
    out,
    eg,
    eu,
    ed,
    sg,
    su,
    sd,
    col_rows,
    col_weights,
    x_send,
    x_recv,
    y_send,
    y_recv,
    p_send,
    p_recv,
    total,
    load_sem,
    own_sem,
    row_s,
    row_r,
    wt_s,
    wt_r,
    x_s,
    x_r,
    y_s,
    y_r,
    p_s,
    p_r,
):
    me = lax.axis_index("ep")
    z = me // width
    p = me % width
    model = normed.shape[1]
    chunk = model // PIECES
    columns = [slice(i * chunk, (i + 1) * chunk) for i in range(PIECES)]
    loads = [
        pltpu.make_async_copy(src, dst, load_sem.at[i])
        for i, (src, dst) in enumerate(
            ((sg_hbm, sg), (su_hbm, su), (sd_hbm, sd), (eg_hbm, eg), (eu_hbm, eu), (ed_hbm, ed))
        )
    ]
    for load in loads:
        load.start()

    barrier = pltpu.get_barrier_semaphore()
    for d in range(1, planes):
        pl.semaphore_signal(
            barrier, inc=1, device_id=(flipped(z, d) * width + p,), device_id_type=MESH
        )
    for r in range(1, width):
        pl.semaphore_signal(
            barrier, inc=1, device_id=(z * width + flipped(p, r),), device_id_type=MESH
        )
    pl.semaphore_wait(barrier, planes - 1 + width - 1)

    sends = []

    def send(src, dst, send_sem, recv_sem, target):
        copy = pltpu.make_async_remote_copy(
            src_ref=src,
            dst_ref=dst,
            send_sem=send_sem,
            recv_sem=recv_sem,
            device_id=(target,),
            device_id_type=MESH,
        )
        copy.start()
        sends.append(copy)

    def part(buf, d, q, i):
        return buf.at[d, pl.ds(pl.multiple_of(q * cap, cap), cap), columns[i]]

    for d in range(1, planes):
        zt = flipped(z, d)
        target = zt * width + p
        send(slot_weights.at[zt], col_weights.at[d], wt_s.at[d], wt_r.at[d], target)
        for i in range(PIECES):
            send(
                normed.at[:, columns[i]],
                col_rows.at[d, :, columns[i]],
                row_s.at[d, i],
                row_r.at[d, i],
                target,
            )

    def arrive(buf, sem):
        pltpu.make_async_copy(buf, buf, sem).wait()

    def block_weights(d):
        return slot_weights[z] if d == 0 else col_weights[d]

    def exchange(src, dst, d, i, send_sems, recv_sems, own):
        for r in range(1, width):
            q = flipped(p, r)
            send(
                part(src, d, q, i),
                part(dst, d, p, i),
                send_sems.at[d, r, i],
                recv_sems.at[d, r, i],
                z * width + q,
            )
        pltpu.make_async_copy(part(src, d, p, i), part(dst, d, p, i), own).start()

    def gathered(src, dst, d, i, recv_sems, own):
        for r in range(1, width):
            arrive(part(dst, d, flipped(p, r), i), recv_sems.at[d, r, i])
        pltpu.make_async_copy(part(src, d, p, i), part(dst, d, p, i), own).wait()

    def dispatch(d, i):
        if d:
            if i == 0:
                arrive(col_weights.at[d], wt_r.at[d])
            arrive(col_rows.at[d, :, columns[i]], row_r.at[d, i])
        picks = jnp.where(block_weights(d).T > 0.0, 1.0, 0.0).astype(jnp.bfloat16)
        rows = normed[:, columns[i]] if d == 0 else col_rows[d, :, columns[i]]
        x_send[d, :, columns[i]] = jnp.dot(
            picks, rows, preferred_element_type=jnp.float32
        ).astype(jnp.bfloat16)
        exchange(x_send, x_recv, d, i, x_s, x_r, own_sem.at[0, d, i])

    def hidden(rows, w_gate, w_up):
        gate_part = jnp.dot(rows, w_gate[...], preferred_element_type=jnp.float32)
        up_part = jnp.dot(rows, w_up[...], preferred_element_type=jnp.float32)
        return (jax.nn.silu(gate_part) * up_part).astype(jnp.bfloat16)

    def expert(d):
        for i in range(PIECES):
            gathered(x_send, x_recv, d, i, x_r, own_sem.at[0, d, i])
        if d == 0:
            for load in loads[3:]:
                load.wait()
        mid = hidden(x_recv[d], eg, eu)
        for i in range(PIECES):
            y_send[d, :, columns[i]] = jnp.dot(
                mid, ed[:, columns[i]], preferred_element_type=jnp.float32
            ).astype(jnp.bfloat16)
            exchange(y_send, y_recv, d, i, y_s, y_r, own_sem.at[1, d, i])

    def combine(d):
        weights = block_weights(d)
        high = weights.astype(jnp.bfloat16)
        low = (weights - high.astype(jnp.float32)).astype(jnp.bfloat16)
        for i in range(PIECES):
            gathered(y_send, y_recv, d, i, y_r, own_sem.at[1, d, i])
            rows = y_recv[d, :, columns[i]]
            partial = jnp.dot(high, rows, preferred_element_type=jnp.float32) + jnp.dot(
                low, rows, preferred_element_type=jnp.float32
            )
            if d == 0:
                total[:, columns[i]] += partial
            else:
                p_send[d, :, columns[i]] = partial.astype(jnp.bfloat16)
                send(
                    p_send.at[d, :, columns[i]],
                    p_recv.at[d, :, columns[i]],
                    p_s.at[d, i],
                    p_r.at[d, i],
                    flipped(z, d) * width + p,
                )

    for i in range(PIECES):
        dispatch(0, i)
    for load in loads[:3]:
        load.wait()
    mid = hidden(normed[...], sg, su)
    for i in range(PIECES):
        total[:, columns[i]] = jnp.dot(
            mid, sd[:, columns[i]], preferred_element_type=jnp.float32
        )
    last = planes - 1
    for d in range(1, planes):
        for i in range(PIECES):
            dispatch(d, i)
            if i == 0 and d > 1 and d < last:
                expert(d - 1)
        if d == 1:
            expert(0)
    if last > 1:
        expert(last - 1)
    for d in range(1, last - 1):
        combine(d)
    if last > 0:
        expert(last)
    if last > 1:
        combine(last - 1)
    combine(0)
    if last > 0:
        combine(last)
    for d in range(1, planes):
        for i in range(PIECES):
            arrive(p_recv.at[d, :, columns[i]], p_r.at[d, i])
    combined = total[...]
    for d in range(1, planes):
        combined = combined + p_recv[d].astype(jnp.float32)
    out[...] = (
        resid[...].astype(jnp.float32) + scaled_norm(combined, out_gain[...])
    ).astype(out.dtype)
    for copy in sends:
        copy.wait_send()


def moe_layer(
    normed, resid_mid, slot_weights, moe_out_gain, experts, shared_weights, planes, width, cap
):
    seq_count, model = normed.shape
    half = jnp.bfloat16
    vmem = pl.BlockSpec(memory_space=pltpu.VMEM)
    hbm = pl.BlockSpec(memory_space=pl.ANY)
    slots = (planes, width * cap, model)
    dense = (planes, seq_count, model)
    dma = pltpu.SemaphoreType.DMA
    weights = (*experts, *shared_weights)
    return pl.pallas_call(
        functools.partial(moe_kernel, planes, width, cap),
        out_shape=jax.ShapeDtypeStruct((seq_count, model), half),
        in_specs=[vmem] * 4 + [hbm] * 6,
        out_specs=vmem,
        scratch_shapes=[pltpu.VMEM(w.shape, w.dtype) for w in weights]
        + [
            pltpu.VMEM(dense, half),
            pltpu.VMEM(slot_weights.shape, jnp.float32),
            pltpu.VMEM(slots, half),
            pltpu.VMEM(slots, half),
            pltpu.VMEM(slots, half),
            pltpu.VMEM(slots, half),
            pltpu.VMEM(dense, half),
            pltpu.VMEM(dense, half),
            pltpu.VMEM((seq_count, model), jnp.float32),
            dma((6,)),
            dma((2, planes, PIECES)),
            dma((planes, PIECES)),
            dma((planes, PIECES)),
            dma((planes,)),
            dma((planes,)),
            *[dma((planes, width, PIECES))] * 4,
            dma((planes, PIECES)),
            dma((planes, PIECES)),
        ],
        compiler_params=pltpu.CompilerParams(
            collective_id=0, has_side_effects=True, vmem_limit_bytes=60 * 1024 * 1024
        ),
        name="moe_exchange",
    )(normed, resid_mid, slot_weights, moe_out_gain[None, :], *weights)


def slot_table(routes, route_weights, planes, width, cap):
    seq_count, top_count = routes.shape
    columns = planes * width * cap
    column = jnp.arange(columns, dtype=jnp.int32)
    column_expert = (column // cap).reshape(planes, 1, width * cap)
    column_slot = (column % cap).reshape(planes, 1, width * cap)
    match = routes.T[:, None, :, None] == column_expert[None]
    chosen = jnp.any(match, axis=0)
    weight = jnp.sum(jnp.where(match, route_weights.T[:, None, :, None], 0.0), axis=0)
    earlier = jnp.tril(jnp.ones((seq_count, seq_count), jnp.bfloat16), -1)
    rank = jnp.einsum(
        "ut,ztj->zuj", earlier, chosen.astype(jnp.bfloat16), preferred_element_type=jnp.float32
    )
    return jnp.where(chosen & (rank == column_slot.astype(jnp.float32)), weight, 0.0)


def wide(block, groups):
    rows, states = block.shape
    tiled = jnp.concatenate([block] * groups, axis=1)
    shape = (rows, groups * states)
    row = lax.broadcasted_iota(jnp.int32, shape, 0) // (rows // groups)
    column = lax.broadcasted_iota(jnp.int32, shape, 1) // states
    return jnp.where(row == column, tiled, 0.0)


def halves(value):
    high = value.astype(jnp.bfloat16)
    return high, (value - high.astype(jnp.float32)).astype(jnp.bfloat16)


def mixer_kernel(
    groups,
    residual,
    feed,
    state_re,
    state_im,
    abar_re,
    abar_im,
    bbar_re,
    bbar_im,
    out_re,
    out_im,
    skip,
    value_hbm,
    gate_hbm,
    mix_gain,
    in_gain,
    resid_mid,
    normed,
    next_re,
    next_im,
    old_re,
    old_im,
    new_re,
    new_im,
    value,
    gate,
    active,
    in_sem,
    out_sem,
    glu_sem,
):
    states = abar_re.shape[1]
    chans = bbar_re.shape[0] // abar_re.shape[0]
    lanes = groups * states
    feeds = groups * chans
    count = abar_re.shape[0] // groups

    def piece(n):
        return slice(n * lanes, (n + 1) * lanes)

    def read(n):
        return [
            pltpu.make_async_copy(src.at[:, piece(n)], dst.at[:, piece(n)], in_sem.at[k, n])
            for k, (src, dst) in enumerate(((state_re, old_re), (state_im, old_im)))
        ]

    def write(n):
        return [
            pltpu.make_async_copy(src.at[:, piece(n)], dst.at[:, piece(n)], out_sem.at[k, n])
            for k, (src, dst) in enumerate(((new_re, next_re), (new_im, next_im)))
        ]

    glu = [
        pltpu.make_async_copy(value_hbm, value, glu_sem.at[0]),
        pltpu.make_async_copy(gate_hbm, gate, glu_sem.at[1]),
    ]
    for n in range(count):
        for copy in read(n):
            copy.start()
    for copy in glu:
        copy.start()

    nt = (((1,), (1,)), ((), ()))
    for n in range(count):
        rows = slice(n * feeds, (n + 1) * feeds)
        some = slice(n * groups, (n + 1) * groups)
        u = feed[:, rows]
        a_re = jnp.sum(wide(abar_re[some, :], groups), axis=0, keepdims=True)
        a_im = jnp.sum(wide(abar_im[some, :], groups), axis=0, keepdims=True)

        def force(bbar):
            high, low = halves(wide(bbar[rows, :], groups))
            return jnp.dot(u, high, preferred_element_type=jnp.float32) + jnp.dot(
                u, low, preferred_element_type=jnp.float32
            )

        def readout(fresh, matrix):
            weights = wide(matrix[rows, :].astype(jnp.float32), groups).astype(jnp.bfloat16)
            high, low = halves(fresh)
            return lax.dot_general(
                high, weights, nt, preferred_element_type=jnp.float32
            ) + lax.dot_general(low, weights, nt, preferred_element_type=jnp.float32)

        for copy in read(n):
            copy.wait()
        was_re, was_im = old_re[:, piece(n)], old_im[:, piece(n)]
        fresh_re = a_re * was_re - a_im * was_im + force(bbar_re)
        fresh_im = a_re * was_im + a_im * was_re + force(bbar_im)
        new_re[:, piece(n)] = fresh_re
        new_im[:, piece(n)] = fresh_im
        for copy in write(n):
            copy.start()
        mixed = (
            readout(fresh_re, out_re)
            - readout(fresh_im, out_im)
            + skip[:, rows] * u.astype(jnp.float32)
        )
        active[:, rows] = jax.nn.gelu(mixed).astype(jnp.bfloat16)
    for copy in glu:
        copy.wait()
    acts = active[...]
    value_part = jnp.dot(acts, value[...], preferred_element_type=jnp.float32)
    gate_part = jnp.dot(acts, gate[...], preferred_element_type=jnp.float32)
    branch = value_part * jax.nn.sigmoid(gate_part)
    mid = (residual[...].astype(jnp.float32) + scaled_norm(branch, mix_gain[...])).astype(
        jnp.bfloat16
    )
    resid_mid[...] = mid
    normed[...] = scaled_norm(mid.astype(jnp.float32), in_gain[...]).astype(jnp.bfloat16)
    for n in range(count):
        for copy in write(n):
            copy.wait()


def mixer(
    residual,
    branch_in,
    state_real,
    state_imag,
    decay_rate,
    frequency,
    log_step,
    input_real,
    input_imag,
    output_matrix_real,
    output_matrix_imaginary,
    skip_gain,
    glu_value,
    glu_gate,
    mix_gain,
    moe_in_gain,
):
    group_count, state_count = decay_rate.shape
    step_size = jnp.exp(log_step)[:, None]
    magnitude = jnp.exp(-decay_rate * step_size)
    abar_re = magnitude * jnp.cos(frequency * step_size)
    abar_im = magnitude * jnp.sin(frequency * step_size)
    lam_re = -decay_rate
    denominator = lam_re * lam_re + frequency * frequency
    numer_re = abar_re - 1.0
    coef_re = ((numer_re * lam_re + abar_im * frequency) / denominator)[:, None, :]
    coef_im = ((abar_im * lam_re - numer_re * frequency) / denominator)[:, None, :]
    b_real = input_real.astype(jnp.float32).transpose(0, 2, 1)
    b_imag = input_imag.astype(jnp.float32).transpose(0, 2, 1)
    bbar_re = (coef_re * b_real - coef_im * b_imag).reshape(-1, state_count)
    bbar_im = (coef_re * b_imag + coef_im * b_real).reshape(-1, state_count)
    groups = max(1, 128 // input_real.shape[2])
    count = group_count // groups
    vmem = pl.BlockSpec(memory_space=pltpu.VMEM)
    hbm = pl.BlockSpec(memory_space=pl.ANY)
    state = state_real.shape
    rows = jax.ShapeDtypeStruct(residual.shape, jnp.bfloat16)
    dma = pltpu.SemaphoreType.DMA
    return pl.pallas_call(
        functools.partial(mixer_kernel, groups),
        out_shape=(
            rows,
            rows,
            jax.ShapeDtypeStruct(state, jnp.float32),
            jax.ShapeDtypeStruct(state, jnp.float32),
        ),
        in_specs=[vmem, vmem, hbm, hbm] + [vmem] * 7 + [hbm, hbm, vmem, vmem],
        out_specs=(vmem, vmem, hbm, hbm),
        scratch_shapes=[
            *[pltpu.VMEM(state, jnp.float32)] * 4,
            pltpu.VMEM(glu_value.shape, jnp.bfloat16),
            pltpu.VMEM(glu_gate.shape, jnp.bfloat16),
            pltpu.VMEM(branch_in.shape, jnp.bfloat16),
            dma((2, count)),
            dma((2, count)),
            dma((2,)),
        ],
        compiler_params=pltpu.CompilerParams(vmem_limit_bytes=60 * 1024 * 1024),
        name="mixer",
    )(
        residual,
        branch_in,
        state_real,
        state_imag,
        abar_re,
        abar_im,
        bbar_re,
        bbar_im,
        output_matrix_real.reshape(-1, state_count),
        output_matrix_imaginary.reshape(-1, state_count),
        skip_gain[None, :],
        glu_value,
        glu_gate,
        mix_gain[None, :],
        moe_in_gain[None, :],
    )


def serve_rows(
    residual, branch_in, state_real, state_imag, routes, route_weights, params, capacity
):
    (
        decay_rate,
        frequency,
        log_step,
        input_real,
        input_imag,
        output_matrix_real,
        output_matrix_imaginary,
        skip_gain,
        glu_value,
        glu_gate,
        mix_gain,
        moe_in_gain,
        moe_out_gain,
        expert_gate,
        expert_up,
        expert_down,
        shared_gate,
        shared_up,
        shared_down,
    ) = params
    resid_mid, normed, next_real, next_imag = mixer(
        residual,
        branch_in,
        state_real,
        state_imag,
        decay_rate,
        frequency,
        log_step,
        input_real,
        input_imag,
        output_matrix_real,
        output_matrix_imaginary,
        skip_gain,
        glu_value,
        glu_gate,
        mix_gain,
        moe_in_gain,
    )
    count = lax.axis_size("ep")
    cap = -(-capacity // ROW_TILE) * ROW_TILE
    planes = residual.shape[0] // cap
    width = count // planes
    layer_out = moe_layer(
        normed,
        resid_mid,
        slot_table(routes, route_weights, planes, width, cap),
        moe_out_gain,
        (expert_gate[0], expert_up[0], expert_down[0]),
        (shared_gate, shared_up, shared_down),
        planes,
        width,
        cap,
    )
    return (layer_out, next_real, next_imag)


def per_device(
    residual,
    branch_in,
    state_real,
    state_imag,
    decay_rate,
    frequency,
    log_step,
    input_real,
    input_imag,
    output_matrix_real,
    output_matrix_imaginary,
    skip_gain,
    glu_value,
    glu_gate,
    mix_gain,
    moe_in_gain,
    moe_out_gain,
    routes,
    route_weights,
    expert_gate,
    expert_up,
    expert_down,
    shared_gate,
    shared_up,
    shared_down,
):
    params = (
        decay_rate,
        frequency,
        log_step,
        input_real,
        input_imag,
        output_matrix_real,
        output_matrix_imaginary,
        skip_gain,
        glu_value,
        glu_gate,
        mix_gain,
        moe_in_gain,
        moe_out_gain,
        expert_gate,
        expert_up,
        expert_down,
        shared_gate,
        shared_up,
        shared_down,
    )
    seq_dev = residual.shape[0]
    capacity = max(2, 4 * seq_dev * routes.shape[1] // (3 * lax.axis_size("ep")))
    return serve_rows(
        residual, branch_in, state_real, state_imag, routes, route_weights, params, capacity
    )


def solution(mesh):
    return jax.shard_map(
        per_device,
        mesh=mesh,
        in_specs=(
            P("ep", None),
            P("ep", None),
            P("ep", None),
            P("ep", None),
            P(),
            P(),
            P(),
            P(),
            P(),
            P(),
            P(),
            P(),
            P(),
            P(),
            P(),
            P(),
            P(),
            P("ep", None),
            P("ep", None),
            P("ep", None, None),
            P("ep", None, None),
            P("ep", None, None),
            P(),
            P(),
            P(),
        ),
        out_specs=(P("ep", None), P("ep", None), P("ep", None)),
        check_vma=False,
    )
```

profile of v0, /device:TPU:17, one launch (start us, length us, event | category | flops | bytes accessed | tf_op | source)
XLA Modules:
  0.0 92.2 jit_solution(7846614267290480310)
XLA Ops:
  0.6 0.7 exp.6
  1.3 1.6 %add_divide_fusion = (f32[64,64]{1,0:T(8,128)S(1)}, f32[64,64]{1,0:T(8,128)}, f32[64,64]{1,0:T(8,128)S(1)}, f32[64,64]{1,0:T(8,128)}) fusion(f32[64,64]{1,0:T(8,128)} %param.30, f32[64,64]{1,0:T(8,128)} %param.29, f32[64]{0:T(128)S(1)} %exp.6), kind=kLoop, calls=%fused_computation.16 | loop fusion | flops 69632 | bytes 98560 | tf_op jit(solution)/shard_map/div | solution.py:463
  2.9 2.2 %fusion.5 = (f32[64,64,16]{1,2,0:T(8,128)}, f32[64,64,16]{1,2,0:T(8,128)}) fusion(bf16[64,64,16]{1,2,0:T(8,128)(2,1)} %param.32, bf16[64,64,16]{1,2,0:T(8,128)(2,1)} %param.33, f32[64,64]{1,0:T(8,128)S(1)} %get-tuple-element.15, f32[64,64]{1,0:T(8,128)S(1)} %get-tuple-element.13), kind=kLoop, calls=%fused_computation.12 | loop fusion | flops 524288 | bytes 819200 | tf_op jit(solution)/shard_map/add | solution.py:468
  5.1 0.0 copy-start
  5.1 0.0 copy-start.1
  5.1 10.2 %mixer.1 = (bf16[64,2048]{1,0:T(8,128)(2,1)}, bf16[64,2048]{1,0:T(8,128)(2,1)}, f32[64,4096]{1,0:T(8,128)}, f32[64,4096]{1,0:T(8,128)}) custom-call(bf16[64,2048]{1,0:T(8,128)(2,1)} %residual.1, bf16[64,1024]{1,0:T(8,128)(2,1)} %feed.1, f32[64,4096]{1,0:T(8,128)} %state_re.1, f32[64,4096]{1,0:T(8,128)} %state_im.1, f32[64,64]{1,0:T(8,128)} %get-tuple-element.14.abar_re, ...), custom_call_target="tpu_custom_call" | custom-call | tf_op jit(solution)/shard_map/mixer/pallas_call | solution.py:476
  15.3 0.0 copy-done
  15.3 0.0 copy-done.1
  15.3 0.2 fusion.3
  15.5 0.2 compare_reduce_fusion
  15.7 0.9 fusion.2.slot_weights
  16.5 74.0 %moe_exchange.1 = bf16[64,2048]{1,0:T(8,128)(2,1)} custom-call(bf16[64,2048]{1,0:T(8,128)(2,1)} %get-tuple-element.7.normed, bf16[64,2048]{1,0:T(8,128)(2,1)} %get-tuple-element.8.resid, f32[4,64,128]{2,1,0:T(8,128)} %fusion.2.slot_weights, f32[1,2048]{1,0:T(1,128)} %bitcast.38, bf16[2048,512]{1,0:T(8,128)(2,1)} %bitcast.29, bf16[2048,512]{1,0:T(8,128)(2,1)} %bitcast.30, ...), custom_call_target="tpu_custom_call" | custom-call | tf_op jit(solution)/shard_map/moe_exchange/pallas_call | solution.py:259
  90.5 1.7 %copy.29 = bf16[64,2048]{1,0:T(8,128)(2,1)} copy(bf16[64,2048]{1,0:T(8,128)(2,1)} %moe_exchange.1) | data formatting | bytes 524288
  (3 shorter events, 0.0 us)
Async XLA Ops:
  5.1 10.2 %copy-start = (s32[64,6]{0,1:T(8,128)S(1)}, s32[64,6]{0,1:T(8,128)}, u32[]{:S(2)}) copy-start(s32[64,6]{0,1:T(8,128)} %param.42) | copy-start | bytes 4612
  5.1 10.2 %copy-start.1 = (f32[64,6]{0,1:T(8,128)S(1)}, f32[64,6]{0,1:T(8,128)}, u32[]{:S(2)}) copy-start(f32[64,6]{0,1:T(8,128)} %param.43) | copy-start | bytes 4612
where the time goes:
time: 92.5 us; the launch traced here: 92.2 us
  Pallas kernels  84.2 us (91%)
  other arithmetic  4.13 us (4%)
  local copies, waits for them, and re-layouts  2.34 us (3%)
    pallas_call x1, Pallas kernels, moe_layer(): pl.pallas_call(functools.partial(moe_kernel, planes, width, cap), out_sha...  74 us
    pallas_call x1, Pallas kernels, mixer(): pl.pallas_call(functools.partial(mixer_kernel, groups), out_shape=(rows,...  10.2 us
    add x1, other arithmetic, mixer(): bbar_im = (coef_re * b_imag + coef_im * b_real).reshape(-1, state_count)  2.16 us

commit v1 on v0

v1 whole, which is shorter than its diff:
```python
import functools
import math

import jax
import jax.numpy as jnp
from jax import lax
from jax.experimental import pallas as pl
from jax.experimental.pallas import tpu as pltpu
from jax.sharding import PartitionSpec as P

norm_eps = 1e-06
ROW_TILE = 16
PIECES = 2
STRIPS = 4
WINDOW = 2
AHEAD = 3
LAG = 1
VMEM_MOST = 60 * 1024 * 1024
SPARE = 8 * 1024 * 1024
MESH = pl.DeviceIdType.MESH


def scaled_norm(row_block, norm_gain):
    return (
        row_block
        * lax.rsqrt(jnp.mean(row_block * row_block, axis=-1, keepdims=True) + norm_eps)
        * norm_gain
    )


def in_hbm(*arrays):
    return [pltpu.with_memory_space_constraint(array, pltpu.HBM) for array in arrays]


def flipped(index, mask):
    out, bit = 0, 1
    while bit <= mask or bit == 1:
        digit = (index // bit) % 2
        out = out + bit * ((digit + 1) % 2 if mask & bit else digit)
        bit *= 2
    return out + (index // bit) * bit


def pick_from(table, z, k):
    value, planes = 0, len(table)
    for row in range(planes):
        away = ((z - row + planes) % planes + planes - 1) // planes
        value = value + table[row][k] * (1 - away)
    return value


def block_order(planes):
    half = max(1, planes // 2)
    order = []
    for z in range(planes):
        others = [b for b in range(planes) if b != z]
        order.append([z] + sorted(others, key=lambda b: (b // half != z // half, abs(b - z), b)))
    return order


def moe_kernel(
    planes,
    width,
    cap,
    top,
    normed,
    resid,
    out_gain_hbm,
    eg_hbm,
    eu_hbm,
    ed_hbm,
    sg_hbm,
    su_hbm,
    sd_hbm,
    out,
    eg,
    eu,
    ed,
    sg,
    su,
    sd,
    out_gain,
    col_rows,
    mix,
    x_send,
    x_recv,
    y_send,
    y_recv,
    part,
    p_send,
    q_recv,
    total,
    load_sem,
    z_s,
    row_r,
    x_s,
    x_r,
    y_s,
    y_r,
    p_s,
    q_r,
):
    me = lax.axis_index("ep")
    z = me // width
    p = me % width
    seq, model = resid.shape
    head = normed.shape[1] - model
    pad = -(-top // 8) * 8
    slots = width * cap
    chunk = model // PIECES
    columns = [slice(i * chunk, (i + 1) * chunk) for i in range(PIECES)]
    pieces = range(PIECES)
    last = planes - 1
    strip = model // STRIPS
    order = block_order(planes)
    upward = [[int(b > r) for b in order[r]] for r in range(planes)]
    behind = [[int(r > 0 if b > r else r < last) for b in order[r]] for r in range(planes)]
    block = [pick_from(order, z, k) for k in range(planes)]

    loads = [
        pltpu.make_async_copy(src, dst, load_sem.at[i])
        for i, (src, dst) in enumerate(
            (
                (sg_hbm, sg),
                (su_hbm, su),
                (sd_hbm, sd),
                (eg_hbm, eg),
                (eu_hbm, eu),
                (ed_hbm, ed),
                (out_gain_hbm, out_gain),
            )
        )
    ]
    for load in (*loads[6:], *loads[:6]):
        load.start()

    barrier = pltpu.get_barrier_semaphore()
    sides = ((z > 0, -1), (z < last, 1)) if planes > 1 else ()
    for there, step in sides:

        @pl.when(there)
        def _():
            pl.semaphore_signal(
                barrier, inc=1, device_id=((z + step) * width + p,), device_id_type=MESH
            )

    for r in range(1, width):
        pl.semaphore_signal(
            barrier, inc=1, device_id=(z * width + flipped(p, r),), device_id_type=MESH
        )

    x_ends, ends = [], []

    def send(src, dst, send_sem, recv_sem, target, kept):
        copy = pltpu.make_async_remote_copy(
            src_ref=src,
            dst_ref=dst,
            send_sem=send_sem,
            recv_sem=recv_sem,
            device_id=(target,),
            device_id_type=MESH,
        )
        copy.start()
        kept.append(copy)

    def arrive(buf, sem):
        pltpu.make_async_copy(buf, buf, sem).wait()

    def part_of(buf, k, q, i):
        return buf.at[k, pl.ds(pl.multiple_of(q * cap, cap), cap), columns[i]]

    def table(k):
        rows = normed[:, :head] if k == 0 else col_rows[block[k], :, :head]
        seen = rows.astype(jnp.float32).T
        slot = lax.broadcasted_iota(jnp.int32, (slots, seq), 0)
        expert = (z * width + slot // cap).astype(jnp.float32)
        chosen = jnp.zeros((slots, seq), jnp.float32)
        weight = jnp.zeros((slots, seq), jnp.float32)

        def line(group, j):
            return seen[group * pad + j : group * pad + j + 1, :]

        for j in range(top):
            hit = line(0, j) * 256.0 + line(1, j) == expert
            chosen = jnp.where(hit, 1.0, chosen)
            weight = jnp.where(hit, line(2, j) + line(3, j) + line(4, j), weight)
        earlier = jnp.where(
            lax.broadcasted_iota(jnp.int32, (seq, seq), 0)
            < lax.broadcasted_iota(jnp.int32, (seq, seq), 1),
            1.0,
            0.0,
        ).astype(jnp.bfloat16)
        rank = jnp.dot(chosen.astype(jnp.bfloat16), earlier, preferred_element_type=jnp.float32)
        place = (slot % cap).astype(jnp.float32)
        picks = jnp.where(rank == place, chosen, 0.0)
        spread = (picks * weight).T
        high = spread.astype(jnp.bfloat16)
        mix[k, :seq] = high
        mix[k, seq:] = (spread - high.astype(jnp.float32)).astype(jnp.bfloat16)
        return picks.astype(jnp.bfloat16)

    def gather(k, i, picks):
        span = slice(head + i * chunk, head + (i + 1) * chunk)
        rows = normed[:, span] if k == 0 else col_rows[block[k], :, span]
        x_send[k, :, columns[i]] = jnp.dot(
            picks, rows, preferred_element_type=jnp.float32
        ).astype(jnp.bfloat16)

    def exchange(src, dst, k, i, send_sems, recv_sems, kept):
        for r in range(1, width):
            q = flipped(p, r)
            send(
                part_of(src, k, q, i),
                part_of(dst, k, p, i),
                send_sems.at[k, r, i],
                recv_sems.at[k, r, i],
                z * width + q,
                kept,
            )
        mine = pl.ds(pl.multiple_of(p * cap, cap), cap)
        dst[k, mine, columns[i]] = src[k, mine, columns[i]]

    def gathered(dst, k, i, recv_sems):
        for r in range(1, width):
            arrive(part_of(dst, k, flipped(p, r), i), recv_sems.at[k, r, i])

    def z_piece(ref, j):
        return ref.at[:, slice(head + j * strip if j else 0, head + (j + 1) * strip)]

    def z_copy(s, f, j):
        source = (z - f + planes) % planes if s == 0 else (z + f) % planes
        buf = col_rows.at[source]
        return pltpu.make_async_remote_copy(
            src_ref=z_piece(buf if f else normed, j),
            dst_ref=z_piece(buf, j),
            send_sem=z_s.at[s, f, j],
            recv_sem=row_r.at[source, j],
            device_id=((z + 1 - 2 * s + planes) % planes * width + p,),
            device_id_type=MESH,
        )

    def moves(s, f):
        return [int(r >= f and r < last) if s == 0 else int(r <= last - f and r > 0) for r in range(planes)]

    def z_sent(s, f, j):
        z_copy(s, f, j).wait_send()

    def z_issue(s, f, j):
        def go():
            before = f * STRIPS + j - WINDOW
            if before >= 0:
                z_sent(s, before // STRIPS, before % STRIPS)
            z_copy(s, f, j).start()

        if any(moves(s, f)):
            pl.when(pick_from([[m] for m in moves(s, f)], z, 0) == 1)(go)

    def z_step(f, j):
        for s in range(2):
            if f:
                source = (z - f + planes) % planes if s == 0 else (z + f) % planes

                @pl.when(z >= f if s == 0 else z <= last - f)
                def _():
                    arrive(z_piece(col_rows.at[source], j), row_r.at[source, j])

            z_issue(s, f, j)

    def z_drain():
        for s in range(2):
            for f in range(planes):
                for j in range(STRIPS):
                    after = (f * STRIPS + j + WINDOW) // STRIPS
                    later = moves(s, after) if after < planes else [0] * planes
                    still = [m * (1 - n) for m, n in zip(moves(s, f), later)]
                    if any(still):
                        pl.when(pick_from([[m] for m in still], z, 0) == 1)(
                            functools.partial(z_sent, s, f, j)
                        )

    def dispatch(k, i, picks):
        gather(k, i, picks)
        exchange(x_send, x_recv, k, i, x_s, x_r, x_ends)

    def hidden(rows, w_gate, w_up):
        gate_part = jnp.dot(rows, w_gate[...], preferred_element_type=jnp.float32)
        up_part = jnp.dot(rows, w_up[...], preferred_element_type=jnp.float32)
        return (jax.nn.silu(gate_part) * up_part).astype(jnp.bfloat16)

    def expert(k):
        for i in pieces:
            gathered(x_recv, k, i, x_r)
        if k == 0:
            for load in loads[3:6]:
                load.wait()
        mid = hidden(x_recv[k], eg, eu)
        for i in pieces:
            y_send[k, :, columns[i]] = jnp.dot(
                mid, ed[:, columns[i]], preferred_element_type=jnp.float32
            ).astype(jnp.bfloat16)

    def give(k, i):
        exchange(y_send, y_recv, k, i, y_s, y_r, ends)

    def landed(k, i):
        gathered(y_recv, k, i, y_r)

    def weighed(k, i):
        both = jnp.dot(mix[k], y_recv[k, :, columns[i]], preferred_element_type=jnp.float32)
        return both[:seq] + both[seq:]

    def lane(j):
        return slice(j * strip, (j + 1) * strip)

    def strips_of(i):
        return range(i * STRIPS // PIECES, (i + 1) * STRIPS // PIECES)

    def passed_copy(k, j):
        up = pick_from(upward, z, k)
        return pltpu.make_async_remote_copy(
            src_ref=p_send.at[k, :, lane(j)],
            dst_ref=q_recv.at[1 - up, block[k], :, lane(j)],
            send_sem=p_s.at[k, j],
            recv_sem=q_r.at[1 - up, block[k], j],
            device_id=((z - 1 + 2 * up) * width + p,),
            device_id_type=MESH,
        )

    def combine(k, i):
        value = weighed(k, i)
        if k == 0:
            total[:, columns[i]] += value
            return
        part[k, :, columns[i]] = value

        @pl.when(pick_from(behind, z, k) == 0)
        def _():
            for j in strips_of(i):
                p_send[k, :, lane(j)] = part[k, :, lane(j)].astype(jnp.bfloat16)
                passed_copy(k, j).start()

    def merge(k, i):
        up = pick_from(upward, z, k)

        @pl.when(pick_from(behind, z, k) == 1)
        def _():
            for j in strips_of(i):
                landed = q_recv.at[1 - up, block[k], :, lane(j)]
                arrive(landed, q_r.at[1 - up, block[k], j])
                p_send[k, :, lane(j)] = (
                    part[k, :, lane(j)]
                    + q_recv[1 - up, block[k], :, lane(j)].astype(jnp.float32)
                ).astype(jnp.bfloat16)
                passed_copy(k, j).start()

    picks = table(0)
    for i in pieces:
        gather(0, i, picks)

    greeted = [[int(r > 0) + int(r < last)] for r in range(planes)]
    pl.semaphore_wait(barrier, width - 1 + pick_from(greeted, z, 0))
    for j in range(min(WINDOW, STRIPS)):
        z_step(0, j)
    for i in pieces:
        exchange(x_send, x_recv, 0, i, x_s, x_r, x_ends)

    for load in loads[:3]:
        load.wait()
    mid = hidden(normed[:, head:], sg, su)
    for i in pieces:
        total[:, columns[i]] = jnp.dot(
            mid, sd[:, columns[i]], preferred_element_type=jnp.float32
        )
    for j in range(min(WINDOW, STRIPS), STRIPS):
        z_step(0, j)
    for k in range(1, planes):
        for i in pieces:
            for j in strips_of(i):
                z_step(k, j)
            if i == 0:
                picks = table(k)
            dispatch(k, i, picks)
        expert(k - 1)
    turns = [(k, i) for k in (*range(last, 0, -1), 0) for i in pieces]
    if planes > 2:
        turns.remove((1, 0))
        turns.insert(0, (1, 0))
        give(1, 0)
    final_own = max((n for n, turn in enumerate(turns) if turn[0] == 1), default=-1)
    expert(last)
    for turn in turns[planes > 2 : AHEAD]:
        give(*turn)
    for copy in x_ends:
        copy.wait_send()
    done = []
    for n, turn in enumerate(turns):
        landed(*turn)
        if n + AHEAD < len(turns):
            give(*turns[n + AHEAD])
        combine(*turn)
        if turn[0] > 1:
            done.append(turn)
        if turn[0] > 1 and len(done) > LAG:
            merge(*done.pop(0))
        if n == final_own:
            for late in ((1, 0), *done, *((1, i) for i in pieces[1:])):
                merge(*late)
    for side, (there, _) in enumerate(sides):

        @pl.when(there)
        def _():
            for i in pieces:
                for j in strips_of(i):
                    arrive(q_recv.at[side, z, :, lane(j)], q_r.at[side, z, j])
                total[:, columns[i]] += q_recv[side, z, :, columns[i]].astype(jnp.float32)

    loads[6].wait()
    combined = total[...]
    out[...] = (
        resid[...].astype(jnp.float32) + scaled_norm(combined, out_gain[...])
    ).astype(out.dtype)
    for copy in ends:
        copy.wait_send()
    for k in range(1, planes):
        for j in range(STRIPS):
            passed_copy(k, j).wait_send()
    z_drain()


def moe_layer(
    normed,
    resid_mid,
    top,
    moe_out_gain,
    experts,
    shared_weights,
    planes,
    width,
    cap,
):
    seq_count, model = resid_mid.shape
    half_type = jnp.bfloat16
    vmem = pl.BlockSpec(memory_space=pltpu.VMEM)
    hbm = pl.BlockSpec(memory_space=pltpu.HBM)
    slots = (planes, width * cap, model)
    dense = (planes, seq_count, model)
    dma = pltpu.SemaphoreType.DMA
    weights = (*experts, *shared_weights)
    small = (moe_out_gain[None, :],)
    buffers = [(w.shape, w.dtype) for w in (*weights, *small)] + [
        ((planes, *normed.shape), half_type),
        ((planes, 2 * seq_count, width * cap), half_type),
        (slots, half_type),
        (slots, half_type),
        (slots, half_type),
        (slots, half_type),
        (dense, jnp.float32),
        (dense, half_type),
        ((2, *dense), half_type),
        ((seq_count, model), jnp.float32),
    ]
    used = sum(math.prod(shape) * jnp.dtype(kind).itemsize for shape, kind in buffers)
    return pl.pallas_call(
        functools.partial(moe_kernel, planes, width, cap, top),
        out_shape=jax.ShapeDtypeStruct((seq_count, model), half_type),
        in_specs=[vmem] * 2 + [hbm] * 7,
        out_specs=vmem,
        scratch_shapes=[pltpu.VMEM(shape, kind) for shape, kind in buffers]
        + [
            dma((7,)),
            dma((2, planes, STRIPS)),
            dma((planes, STRIPS)),
            *[dma((planes, width, PIECES))] * 4,
            dma((planes, STRIPS)),
            dma((2, planes, STRIPS)),
        ],
        compiler_params=pltpu.CompilerParams(
            collective_id=0,
            has_side_effects=True,
            vmem_limit_bytes=min(VMEM_MOST, used + SPARE),
        ),
        name="moe_exchange",
    )(normed, resid_mid, *in_hbm(*small, *weights))


def spread(block, groups, mask):
    return jnp.concatenate([block] * groups, axis=1) * mask


def halves(value):
    high = value.astype(jnp.bfloat16)
    return high, (value - high.astype(jnp.float32)).astype(jnp.bfloat16)


def group_mask(rows, groups, states):
    shape = (rows, groups * states)
    row = lax.broadcasted_iota(jnp.int32, shape, 0) // (rows // groups)
    column = lax.broadcasted_iota(jnp.int32, shape, 1) // states
    return jnp.where(row == column, 1.0, 0.0)


def mixer_kernel(groups, names, *refs):
    count_in = len(names) + 4
    given, rest = refs[:count_in], refs[count_in:]
    state_re, state_im, value_hbm, gate_hbm = given[len(names) :]
    resid_mid, normed, next_re, next_im = rest[:4]
    old_re, old_im, new_re, new_im, value, gate, active = rest[4:11]
    held = dict(zip(names, rest[11 : 11 + len(names)]))
    small_sem, in_sem, out_sem, glu_sem = rest[11 + len(names) :]
    small = {
        name: pltpu.make_async_copy(src, held[name], small_sem.at[i])
        for i, (name, src) in enumerate(zip(names, given))
    }
    decay, frequency, log_step = held["decay"], held["frequency"], held["log_step"]
    in_re, in_im, out_re, out_im = (held[m] for m in ("in_re", "in_im", "out_re", "out_im"))
    residual, feed, skip = held["residual"], held["feed"], held["skip"]
    mix_gain, in_gain = held["mix_gain"], held["in_gain"]
    group_count, states = decay.shape
    chans = in_re.shape[0] // group_count
    lanes = groups * states
    feeds = groups * chans
    count = group_count // groups

    def piece(n):
        return slice(n * lanes, (n + 1) * lanes)

    def read(n):
        return [
            pltpu.make_async_copy(src.at[:, piece(n)], dst.at[:, piece(n)], in_sem.at[k, n])
            for k, (src, dst) in enumerate(((state_re, old_re), (state_im, old_im)))
        ]

    def write(n):
        return [
            pltpu.make_async_copy(src.at[:, piece(n)], dst.at[:, piece(n)], out_sem.at[k, n])
            for k, (src, dst) in enumerate(((new_re, next_re), (new_im, next_im)))
        ]

    glu = [
        pltpu.make_async_copy(value_hbm, value, glu_sem.at[0]),
        pltpu.make_async_copy(gate_hbm, gate, glu_sem.at[1]),
    ]
    late = ("residual", "mix_gain", "in_gain")
    early = ("log_step", "decay", "frequency", "routes", "route_weights")
    for name in names:
        if name not in late:
            small[name].start()
    for n in range(count):
        for copy in read(n):
            copy.start()
    for copy in glu:
        copy.start()
    for name in late:
        small[name].start()

    for name in ("log_step", "decay", "frequency"):
        small[name].wait()
    square = (group_count, group_count)
    diagonal = lax.broadcasted_iota(jnp.int32, square, 0) == lax.broadcasted_iota(
        jnp.int32, square, 1
    )
    step_size = jnp.exp(
        jnp.sum(jnp.where(diagonal, log_step[...], 0.0), axis=1, keepdims=True)
    )
    rate, speed = decay[...], frequency[...]
    magnitude = jnp.exp(-rate * step_size)
    abar_re = magnitude * jnp.cos(speed * step_size)
    abar_im = magnitude * jnp.sin(speed * step_size)
    denominator = rate * rate + speed * speed
    numer_re = abar_re - 1.0
    coef_re = (abar_im * speed - numer_re * rate) / denominator
    coef_im = (-abar_im * rate - numer_re * speed) / denominator

    for name in ("routes", "route_weights"):
        small[name].wait()
    head = normed.shape[1] - resid_mid.shape[1]
    chosen, weight = held["routes"][...], held["route_weights"][...]
    top, seq = chosen.shape
    rest_of = -(-top // 8) * 8 - top
    upper, lower = halves(weight)
    lowest = weight - upper.astype(jnp.float32) - lower.astype(jnp.float32)
    parts = []
    for item in (chosen // 256, chosen % 256, upper, lower, lowest):
        parts += [item.astype(jnp.float32)] + [jnp.zeros((rest_of, seq), jnp.float32)] * (rest_of > 0)
    lines = jnp.concatenate(parts, axis=0)
    lines = jnp.concatenate([lines, jnp.zeros((head - lines.shape[0], seq), jnp.float32)], axis=0)
    normed[:, :head] = lines.T.astype(jnp.bfloat16)

    few = group_mask(groups, groups, states)
    many = group_mask(feeds, groups, states).astype(jnp.bfloat16)
    minus = -many
    nt = (((1,), (1,)), ((), ()))

    for name in names:
        if name not in late and name not in early:
            small[name].wait()
    for n in range(count):
        rows = slice(n * feeds, (n + 1) * feeds)
        some = slice(n * groups, (n + 1) * groups)
        u = feed[:, rows]

        def line(block):
            return jnp.sum(spread(block[some, :], groups, few), axis=0, keepdims=True)

        a_re, a_im, c_re, c_im = line(abar_re), line(abar_im), line(coef_re), line(coef_im)
        drive_re = jnp.dot(
            u, spread(in_re[rows, :], groups, many), preferred_element_type=jnp.float32
        )
        drive_im = jnp.dot(
            u, spread(in_im[rows, :], groups, many), preferred_element_type=jnp.float32
        )
        weights = jnp.concatenate(
            [spread(out_re[rows, :], groups, many), spread(out_im[rows, :], groups, minus)],
            axis=1,
        )
        for copy in read(n):
            copy.wait()
        was_re, was_im = old_re[:, piece(n)], old_im[:, piece(n)]
        fresh_re = a_re * was_re - a_im * was_im + (c_re * drive_re - c_im * drive_im)
        fresh_im = a_re * was_im + a_im * was_re + (c_re * drive_im + c_im * drive_re)
        new_re[:, piece(n)] = fresh_re
        new_im[:, piece(n)] = fresh_im
        for copy in write(n):
            copy.start()
        fresh = jnp.concatenate(
            [fresh_re.astype(jnp.bfloat16), fresh_im.astype(jnp.bfloat16)], axis=1
        )
        mixed = lax.dot_general(
            fresh, weights, nt, preferred_element_type=jnp.float32
        ) + skip[:, rows] * u.astype(jnp.float32)
        active[:, rows] = jax.nn.gelu(mixed).astype(jnp.bfloat16)
    for copy in glu:
        copy.wait()
    for name in late:
        small[name].wait()
    acts = active[...]
    value_part = jnp.dot(acts, value[...], preferred_element_type=jnp.float32)
    gate_part = jnp.dot(acts, gate[...], preferred_element_type=jnp.float32)
    branch = value_part * jax.nn.sigmoid(gate_part)
    mid = (residual[...].astype(jnp.float32) + scaled_norm(branch, mix_gain[...])).astype(
        jnp.bfloat16
    )
    resid_mid[...] = mid
    normed[:, head:] = scaled_norm(mid.astype(jnp.float32), in_gain[...]).astype(jnp.bfloat16)
    for n in range(count):
        for copy in write(n):
            copy.wait()


def mixer(
    residual,
    branch_in,
    state_real,
    state_imag,
    decay_rate,
    frequency,
    log_step,
    input_real,
    input_imag,
    output_matrix_real,
    output_matrix_imaginary,
    skip_gain,
    glu_value,
    glu_gate,
    mix_gain,
    moe_in_gain,
    routes,
    route_weights,
):
    group_count, state_count = decay_rate.shape
    inputs = [m.transpose(0, 2, 1).reshape(-1, state_count) for m in (input_real, input_imag)]
    groups = max(1, 128 // input_real.shape[2])
    count = group_count // groups
    vmem = pl.BlockSpec(memory_space=pltpu.VMEM)
    hbm = pl.BlockSpec(memory_space=pltpu.HBM)
    state = state_real.shape
    rows = jax.ShapeDtypeStruct(residual.shape, jnp.bfloat16)
    dma = pltpu.SemaphoreType.DMA
    small = {
        "log_step": log_step[None, :],
        "decay": decay_rate,
        "frequency": frequency,
        "feed": branch_in,
        "in_re": inputs[0],
        "in_im": inputs[1],
        "out_re": output_matrix_real.reshape(-1, state_count),
        "out_im": output_matrix_imaginary.reshape(-1, state_count),
        "skip": skip_gain[None, :],
        "residual": residual,
        "mix_gain": mix_gain[None, :],
        "in_gain": moe_in_gain[None, :],
        "routes": routes.T,
        "route_weights": route_weights.T,
    }
    head = -(-5 * (-(-routes.shape[1] // 8) * 8) // 128) * 128
    wider = (residual.shape[0], residual.shape[1] + head)
    buffers = [(state, jnp.float32)] * 4 + [
        (glu_value.shape, jnp.bfloat16),
        (glu_gate.shape, jnp.bfloat16),
        (branch_in.shape, jnp.bfloat16),
        *[(array.shape, array.dtype) for array in small.values()],
    ]
    used = sum(math.prod(shape) * jnp.dtype(kind).itemsize for shape, kind in buffers)
    return pl.pallas_call(
        functools.partial(mixer_kernel, groups, tuple(small)),
        out_shape=(
            rows,
            jax.ShapeDtypeStruct(wider, jnp.bfloat16),
            jax.ShapeDtypeStruct(state, jnp.float32),
            jax.ShapeDtypeStruct(state, jnp.float32),
        ),
        in_specs=[hbm] * (len(small) + 4),
        out_specs=(vmem, vmem, hbm, hbm),
        scratch_shapes=[pltpu.VMEM(shape, kind) for shape, kind in buffers]
        + [
            dma((len(small),)),
            dma((2, count)),
            dma((2, count)),
            dma((2,)),
        ],
        compiler_params=pltpu.CompilerParams(vmem_limit_bytes=min(VMEM_MOST, used + SPARE)),
        name="mixer",
    )(*in_hbm(*small.values(), state_real, state_imag, glu_value, glu_gate))


def serve_rows(
    residual, branch_in, state_real, state_imag, routes, route_weights, params, capacity
):
    (
        decay_rate,
        frequency,
        log_step,
        input_real,
        input_imag,
        output_matrix_real,
        output_matrix_imaginary,
        skip_gain,
        glu_value,
        glu_gate,
        mix_gain,
        moe_in_gain,
        moe_out_gain,
        expert_gate,
        expert_up,
        expert_down,
        shared_gate,
        shared_up,
        shared_down,
    ) = params
    resid_mid, normed, next_real, next_imag = mixer(
        residual,
        branch_in,
        state_real,
        state_imag,
        decay_rate,
        frequency,
        log_step,
        input_real,
        input_imag,
        output_matrix_real,
        output_matrix_imaginary,
        skip_gain,
        glu_value,
        glu_gate,
        mix_gain,
        moe_in_gain,
        routes,
        route_weights,
    )
    count = lax.axis_size("ep")
    cap = -(-capacity // ROW_TILE) * ROW_TILE
    planes = residual.shape[0] // cap
    width = count // planes
    layer_out = moe_layer(
        normed,
        resid_mid,
        routes.shape[1],
        moe_out_gain,
        (expert_gate[0], expert_up[0], expert_down[0]),
        (shared_gate, shared_up, shared_down),
        planes,
        width,
        cap,
    )
    return (layer_out, next_real, next_imag)


def per_device(
    residual,
    branch_in,
    state_real,
    state_imag,
    decay_rate,
    frequency,
    log_step,
    input_real,
    input_imag,
    output_matrix_real,
    output_matrix_imaginary,
    skip_gain,
    glu_value,
    glu_gate,
    mix_gain,
    moe_in_gain,
    moe_out_gain,
    routes,
    route_weights,
    expert_gate,
    expert_up,
    expert_down,
    shared_gate,
    shared_up,
    shared_down,
):
    params = (
        decay_rate,
        frequency,
        log_step,
        input_real,
        input_imag,
        output_matrix_real,
        output_matrix_imaginary,
        skip_gain,
        glu_value,
        glu_gate,
        mix_gain,
        moe_in_gain,
        moe_out_gain,
        expert_gate,
        expert_up,
        expert_down,
        shared_gate,
        shared_up,
        shared_down,
    )
    seq_dev = residual.shape[0]
    capacity = max(2, 4 * seq_dev * routes.shape[1] // (3 * lax.axis_size("ep")))
    return serve_rows(
        residual, branch_in, state_real, state_imag, routes, route_weights, params, capacity
    )


def solution(mesh):
    return jax.shard_map(
        per_device,
        mesh=mesh,
        in_specs=(
            P("ep", None),
            P("ep", None),
            P("ep", None),
            P("ep", None),
            P(),
            P(),
            P(),
            P(),
            P(),
            P(),
            P(),
            P(),
            P(),
            P(),
            P(),
            P(),
            P(),
            P("ep", None),
            P("ep", None),
            P("ep", None, None),
            P("ep", None, None),
            P("ep", None, None),
            P(),
            P(),
            P(),
        ),
        out_specs=(P("ep", None), P("ep", None), P("ep", None)),
        check_vma=False,
    )
```

time: 92.5 us -> 70.6 us (0.76)
  the two profiles are of different devices: /device:TPU:17 before, /device:TPU:0 now
where the time goes in v1:
time: 70.6 us; the launch traced here: 70.4 us
  Pallas kernels  69.1 us (98%)
  local copies, waits for them, and re-layouts  0.71 us (1%)
    pallas_call x1, Pallas kernels, moe_layer(): pl.pallas_call(functools.partial(moe_kernel, planes, width, cap, top), ou...  61.3 us
    pallas_call x1, Pallas kernels, mixer(): pl.pallas_call(functools.partial(mixer_kernel, groups, tuple(small)), out...  7.73 us

profile of v1, /device:TPU:0, one launch (start us, length us, event | category | flops | bytes accessed | tf_op | source)
XLA Modules:
  0.0 70.4 jit_solution(17655456534480450365)
XLA Ops:
  0.6 7.7 %mixer.1 = (bf16[64,2048]{1,0:T(8,128)(2,1)S(1)}, bf16[64,2176]{1,0:T(8,128)(2,1)S(1)}, f32[64,4096]{1,0:T(8,128)}, f32[64,4096]{1,0:T(8,128)}) custom-call(f32[1,64]{1,0:T(1,128)} %bitcast.31, f32[64,64]{1,0:T(8,128)} %refs_1_.1, f32[64,64]{1,0:T(8,128)} %refs_2_.1, bf16[64,1024]{1,0:T(8,128)(2,1)} %refs_3_.1, bf16[1024,64]{1,0:T(8,128)(2,1)} %bitcast.21, ...), custom_call_target="tpu_custom_call" | custom-call | tf_op jit(solution)/shard_map/mixer/pallas_call | solution.py:704
  8.4 61.3 %moe_exchange.1 = bf16[64,2048]{1,0:T(8,128)(2,1)S(1)} custom-call(bf16[64,2176]{1,0:T(8,128)(2,1)S(1)} %get-tuple-element.7.normed, bf16[64,2048]{1,0:T(8,128)(2,1)S(1)} %get-tuple-element.8.resid, f32[1,2048]{1,0:T(1,128)} %bitcast.27, bf16[2048,512]{1,0:T(8,128)(2,1)} %bitcast.18, bf16[2048,512]{1,0:T(8,128)(2,1)} %bitcast.19, ...), custom_call_target="tpu_custom_call" | custom-call | tf_op jit(solution)/shard_map/moe_exchange/pallas_call | solution.py:463
  69.7 0.7 %copy.29 = bf16[64,2048]{1,0:T(8,128)(2,1)} copy(bf16[64,2048]{1,0:T(8,128)(2,1)S(1)} %moe_exchange.1) | data formatting | bytes 524288

commit v2 on v1

--- a/solution.py
+++ b/solution.py
@@ -12,7 +12,7 @@
 ROW_TILE = 16
 PIECES = 2
 STRIPS = 4
-WINDOW = 2
+WINDOW = 64
 AHEAD = 3
 LAG = 1
 VMEM_MOST = 60 * 1024 * 1024
@@ -151,7 +151,7 @@
 
     x_ends, ends = [], []
 
-    def send(src, dst, send_sem, recv_sem, target, kept):
+    def send(src, dst, send_sem, recv_sem, target):
         copy = pltpu.make_async_remote_copy(
             src_ref=src,
             dst_ref=dst,
@@ -161,7 +161,6 @@
             device_id_type=MESH,
         )
         copy.start()
-        kept.append(copy)
 
     def arrive(buf, sem):
         pltpu.make_async_copy(buf, buf, sem).wait()
@@ -212,17 +211,25 @@
             send(
                 part_of(src, k, q, i),
                 part_of(dst, k, p, i),
-                send_sems.at[k, r, i],
-                recv_sems.at[k, r, i],
+                send_sems.at[k, i],
+                recv_sems.at[k, i],
                 z * width + q,
-                kept,
             )
+        kept.append((src, k, i, send_sems))
         mine = pl.ds(pl.multiple_of(p * cap, cap), cap)
         dst[k, mine, columns[i]] = src[k, mine, columns[i]]
 
+    def others_of(buf, k, i):
+        return buf.at[k, slice(cap, width * cap), columns[i]]
+
     def gathered(dst, k, i, recv_sems):
-        for r in range(1, width):
-            arrive(part_of(dst, k, flipped(p, r), i), recv_sems.at[k, r, i])
+        if width > 1:
+            arrive(others_of(dst, k, i), recv_sems.at[k, i])
+
+    def settle(kept):
+        for src, k, i, sems in kept:
+            if width > 1:
+                arrive(others_of(src, k, i), sems.at[k, i])
 
     def z_piece(ref, j):
         return ref.at[:, slice(head + j * strip if j else 0, head + (j + 1) * strip)]
@@ -282,22 +289,33 @@
         gather(k, i, picks)
         exchange(x_send, x_recv, k, i, x_s, x_r, x_ends)
 
-    def hidden(rows, w_gate, w_up):
-        gate_part = jnp.dot(rows, w_gate[...], preferred_element_type=jnp.float32)
-        up_part = jnp.dot(rows, w_up[...], preferred_element_type=jnp.float32)
+    def hidden(parts, w_gate, w_up):
+        gate_part = up_part = 0.0
+        for i, rows in enumerate(parts):
+            span = columns[i] if len(parts) > 1 else slice(None)
+            block_rows = rows()
+            gate_part += jnp.dot(block_rows, w_gate[span, :], preferred_element_type=jnp.float32)
+            up_part += jnp.dot(block_rows, w_up[span, :], preferred_element_type=jnp.float32)
         return (jax.nn.silu(gate_part) * up_part).astype(jnp.bfloat16)
 
-    def expert(k):
-        for i in pieces:
-            gathered(x_recv, k, i, x_r)
+    def expert(k, ready=()):
+        def rows_of(i):
+            def rows():
+                gathered(x_recv, k, i, x_r)
+                return x_recv[k, :, columns[i]]
+
+            return rows
+
         if k == 0:
             for load in loads[3:6]:
                 load.wait()
-        mid = hidden(x_recv[k], eg, eu)
+        mid = hidden([rows_of(i) for i in pieces], eg, eu)
         for i in pieces:
             y_send[k, :, columns[i]] = jnp.dot(
                 mid, ed[:, columns[i]], preferred_element_type=jnp.float32
             ).astype(jnp.bfloat16)
+            if (k, i) in ready:
+                give(k, i)
 
     def give(k, i):
         exchange(y_send, y_recv, k, i, y_s, y_r, ends)
@@ -366,7 +384,7 @@
 
     for load in loads[:3]:
         load.wait()
-    mid = hidden(normed[:, head:], sg, su)
+    mid = hidden([lambda: normed[:, head:]], sg, su)
     for i in pieces:
         total[:, columns[i]] = jnp.dot(
             mid, sd[:, columns[i]], preferred_element_type=jnp.float32
@@ -387,11 +405,12 @@
         turns.insert(0, (1, 0))
         give(1, 0)
     final_own = max((n for n, turn in enumerate(turns) if turn[0] == 1), default=-1)
-    expert(last)
-    for turn in turns[planes > 2 : AHEAD]:
-        give(*turn)
-    for copy in x_ends:
-        copy.wait_send()
+    first = turns[planes > 2 : AHEAD]
+    expert(last, first)
+    for turn in first:
+        if turn[0] != last:
+            give(*turn)
+    settle(x_ends)
     done = []
     for n, turn in enumerate(turns):
         landed(*turn)
@@ -419,8 +438,7 @@
     out[...] = (
         resid[...].astype(jnp.float32) + scaled_norm(combined, out_gain[...])
     ).astype(out.dtype)
-    for copy in ends:
-        copy.wait_send()
+    settle(ends)
     for k in range(1, planes):
         for j in range(STRIPS):
             passed_copy(k, j).wait_send()
@@ -470,7 +488,7 @@
             dma((7,)),
             dma((2, planes, STRIPS)),
             dma((planes, STRIPS)),
-            *[dma((planes, width, PIECES))] * 4,
+            *[dma((planes, PIECES))] * 4,
             dma((planes, STRIPS)),
             dma((2, planes, STRIPS)),
         ],

time: 70.6 us -> 66.5 us (0.942)
  Pallas kernels: 69.1 us -> 65 us
    pallas_call x1, Pallas kernels: 61.3 us -> 57.3 us  [moe_layer(): pl.pallas_call(functools.partial(moe_kernel, planes, width, cap, top), ou...]
where the time goes in v2:
time: 66.5 us; the launch traced here: 66.4 us
  Pallas kernels  65 us (98%)
  local copies, waits for them, and re-layouts  0.71 us (1%)
    pallas_call x1, Pallas kernels, moe_layer(): pl.pallas_call(functools.partial(moe_kernel, planes, width, cap, top), ou...  57.3 us
    pallas_call x1, Pallas kernels, mixer(): pl.pallas_call(functools.partial(mixer_kernel, groups, tuple(small)), out...  7.73 us

profile of v2, /device:TPU:0, one launch (start us, length us, event | category | flops | bytes accessed | tf_op | source)
XLA Modules:
  0.0 66.4 jit_solution(5224832249462952455)
XLA Ops:
  0.6 7.7 %mixer.1 = (bf16[64,2048]{1,0:T(8,128)(2,1)S(1)}, bf16[64,2176]{1,0:T(8,128)(2,1)S(1)}, f32[64,4096]{1,0:T(8,128)}, f32[64,4096]{1,0:T(8,128)}) custom-call(f32[1,64]{1,0:T(1,128)} %bitcast.31, f32[64,64]{1,0:T(8,128)} %refs_1_.1, f32[64,64]{1,0:T(8,128)} %refs_2_.1, bf16[64,1024]{1,0:T(8,128)(2,1)} %refs_3_.1, bf16[1024,64]{1,0:T(8,128)(2,1)} %bitcast.21, ...), custom_call_target="tpu_custom_call" | custom-call | tf_op jit(solution)/shard_map/mixer/pallas_call | solution.py:722
  8.4 57.3 %moe_exchange.1 = bf16[64,2048]{1,0:T(8,128)(2,1)S(1)} custom-call(bf16[64,2176]{1,0:T(8,128)(2,1)S(1)} %get-tuple-element.7.normed, bf16[64,2048]{1,0:T(8,128)(2,1)S(1)} %get-tuple-element.8.resid, f32[1,2048]{1,0:T(1,128)} %bitcast.27, bf16[2048,512]{1,0:T(8,128)(2,1)} %bitcast.18, bf16[2048,512]{1,0:T(8,128)(2,1)} %bitcast.19, ...), custom_call_target="tpu_custom_call" | custom-call | tf_op jit(solution)/shard_map/moe_exchange/pallas_call | solution.py:481
  65.7 0.7 %copy.29 = bf16[64,2048]{1,0:T(8,128)(2,1)} copy(bf16[64,2048]{1,0:T(8,128)(2,1)S(1)} %moe_exchange.1) | data formatting | bytes 524288
